TPU v7x, 32 devices: a whole 2x2x4 slice. The times are simulated.
32 devices in a mesh: tp: 8 (over z, x), dp: 4 (over y, core).
Axes of the slice: x: 2, y: 2, z: 4, core: 2. Of those that a mesh axis runs over, the one named last changes fastest.
Arguments:
- tokens: bfloat16 [112, 4096], P('tp', 'dp'), may hold values from -6 to 6
- w_query: bfloat16 [2, 4096, 4096], P(None, 'dp', 'tp'), may hold values from -0.09375 to 0.09375
- w_key: bfloat16 [2, 4096, 4096], P(None, 'dp', 'tp'), may hold values from -0.09375 to 0.09375
- w_value: bfloat16 [2, 4096, 4096], P(None, 'dp', 'tp'), may hold values from -0.09375 to 0.09375
- w_outgate: bfloat16 [2, 4096, 4096], P(None, 'dp', 'tp'), may hold values from -0.09375 to 0.09375
- w_ingate: bfloat16 [2, 4096, 32], P(None, 'dp'), may hold values from -0.09375 to 0.09375
- w_forget: bfloat16 [2, 4096, 32], P(None, 'dp'), may hold values from -0.09375 to 0.09375
- forget_bias: float32 [2, 32], P(None, 'tp'), may hold values from -2 to 3
- head_gain: float32 [2, 32, 128], P(None, 'tp'), may hold values from 0.1 to 1.9
- w_proj: bfloat16 [2, 4096, 4096], P(None, 'tp', 'dp'), may hold values from -0.09375 to 0.09375
- mem_matrix: float32 [2, 112, 32, 128, 128], P(None, 'dp', 'tp'), may hold values from -0.8 to 0.8
- mem_norm: float32 [2, 112, 32, 128], P(None, 'dp', 'tp'), may hold values from -1.2 to 1.2
- mem_max: float32 [2, 112, 32], P(None, 'dp', 'tp'), may hold values from -4 to 4
Outputs:
- result: bfloat16 [112, 4096], P('tp', 'dp')
- new_matrix: float32 [2, 112, 32, 128, 128], P(None, 'dp', 'tp')
- new_norm: float32 [2, 112, 32, 128], P(None, 'dp', 'tp')
- new_max: float32 [2, 112, 32], P(None, 'dp', 'tp')
All inputs are finite; a program needn't handle non-finite values.
Results may differ from a plain program's by a relative error of at most 0.017.
Values may be sent and summed in bfloat16 or wider, within the bound.
A program may use at most 128 MiB of HBM per device.

v0:
```python
import jax
import jax.numpy as jnp
from jax import lax
from jax.sharding import PartitionSpec as P

HEAD = 128
norm_eps = 1e-06
head_eps = 1e-05


def cell_update(queries, key_vecs, values, log_in, log_forget, matrix, normvec, maxval):
    max_next = jnp.maximum(log_forget + maxval, log_in)
    decays = jnp.exp(log_forget + maxval - max_next)
    weight_in = jnp.exp(log_in - max_next)
    matrix_new = (
        decays[..., None, None] * matrix
        + weight_in[..., None, None] * key_vecs[..., :, None] * values[..., None, :]
    )
    norm_new = decays[..., None] * normvec + weight_in[..., None] * key_vecs
    numerator = jnp.einsum("bhd,bhde->bhe", queries, matrix_new, precision=lax.Precision.HIGHEST)
    denominator = jnp.maximum(jnp.abs(jnp.sum(queries * norm_new, axis=-1)), 1.0)
    return (numerator / denominator[..., None], matrix_new, norm_new, max_next)


def head_norm(readout, gain, outgate):
    average = jnp.mean(readout, axis=-1, keepdims=True)
    variance = jnp.mean(jnp.square(readout - average), axis=-1, keepdims=True)
    normed = (readout - average) * lax.rsqrt(variance + head_eps) * gain
    return normed * jax.nn.sigmoid(outgate)


def mix_block(gathered, weights, states):
    w_query, w_key, w_value, w_outgate, w_ingate, w_forget, bias, gain, w_proj = weights
    matrix, normvec, maxval = states
    features = gathered.shape[1] * lax.axis_size("dp")
    squares = jnp.sum(jnp.square(gathered.astype(jnp.float32)), axis=1)
    heads_dev = bias.shape[0]
    head_start = lax.axis_index("tp") * heads_dev
    gate_in = lax.dynamic_slice_in_dim(w_ingate, head_start, heads_dev, 1)
    gate_forget = lax.dynamic_slice_in_dim(w_forget, head_start, heads_dev, 1)
    part_query = jnp.dot(gathered, w_query, preferred_element_type=jnp.float32)
    part_key = jnp.dot(gathered, w_key, preferred_element_type=jnp.float32)
    part_value = jnp.dot(gathered, w_value, preferred_element_type=jnp.float32)
    part_outgate = jnp.dot(gathered, w_outgate, preferred_element_type=jnp.float32)
    part_ingate = jnp.dot(gathered, gate_in, preferred_element_type=jnp.float32)
    part_forget = jnp.dot(gathered, gate_forget, preferred_element_type=jnp.float32)
    rows_dev = gathered.shape[0] // lax.axis_size("dp")
    totals = lax.psum(squares, "dp")
    own_sum = lax.dynamic_slice_in_dim(totals, lax.axis_index("dp") * rows_dev, rows_dev, 0)
    sum_query, sum_key, sum_value, sum_outgate, sum_ingate, sum_forget = (
        lax.psum_scatter(part_query, "dp", scatter_dimension=0, tiled=True),
        lax.psum_scatter(part_key, "dp", scatter_dimension=0, tiled=True),
        lax.psum_scatter(part_value, "dp", scatter_dimension=0, tiled=True),
        lax.psum_scatter(part_outgate, "dp", scatter_dimension=0, tiled=True),
        lax.psum_scatter(part_ingate, "dp", scatter_dimension=0, tiled=True),
        lax.psum_scatter(part_forget, "dp", scatter_dimension=0, tiled=True),
    )
    inv_scale = lax.rsqrt(own_sum / features + norm_eps)[:, None]
    head_shape = (rows_dev, heads_dev, HEAD)
    queries = (sum_query * inv_scale).reshape(head_shape)
    key_vecs = (sum_key * inv_scale * HEAD ** (-0.5)).reshape(head_shape)
    values = (sum_value * inv_scale).reshape(head_shape)
    outgate = (sum_outgate * inv_scale).reshape(head_shape)
    log_in = sum_ingate * inv_scale
    log_forget = jax.nn.log_sigmoid(sum_forget * inv_scale + bias[None, :])
    readout, matrix_new, norm_new, max_next = cell_update(
        queries, key_vecs, values, log_in, log_forget, matrix, normvec, maxval
    )
    hidden = head_norm(readout, gain[None], outgate).reshape(rows_dev, -1).astype(jnp.bfloat16)
    out_partial = jnp.dot(
        lax.all_gather(hidden, "dp", axis=0, tiled=True), w_proj, preferred_element_type=jnp.float32
    )
    return (out_partial, matrix_new, norm_new, max_next)


def on_device(
    tokens,
    w_query,
    w_key,
    w_value,
    w_outgate,
    w_ingate,
    w_forget,
    forget_bias,
    head_gain,
    w_proj,
    mem_matrix,
    mem_norm,
    mem_max,
):
    current = lax.all_gather(tokens, "tp", axis=0, tiled=True)
    matrix_list, norm_list, max_list = ([], [], [])
    block_total = w_query.shape[0]
    result = current
    for block_id in range(block_total):
        weights = (
            w_query[block_id],
            w_key[block_id],
            w_value[block_id],
            w_outgate[block_id],
            w_ingate[block_id],
            w_forget[block_id],
            forget_bias[block_id],
            head_gain[block_id],
            w_proj[block_id],
        )
        out_partial, matrix_out, norm_out, max_out = mix_block(
            current, weights, (mem_matrix[block_id], mem_norm[block_id], mem_max[block_id])
        )
        matrix_list.append(matrix_out)
        norm_list.append(norm_out)
        max_list.append(max_out)
        if block_id + 1 < block_total:
            current = lax.psum(out_partial, "tp").astype(jnp.bfloat16)
        else:
            result = lax.psum_scatter(
                out_partial.astype(jnp.bfloat16), "tp", scatter_dimension=0, tiled=True
            )
    return (result, jnp.stack(matrix_list), jnp.stack(norm_list), jnp.stack(max_list))


def solution(mesh):
    in_specs = (
        P("tp", "dp"),
        P(None, "dp", "tp"),
        P(None, "dp", "tp"),
        P(None, "dp", "tp"),
        P(None, "dp", "tp"),
        P(None, "dp", None),
        P(None, "dp", None),
        P(None, "tp"),
        P(None, "tp", None),
        P(None, "tp", "dp"),
        P(None, "dp", "tp", None, None),
        P(None, "dp", "tp", None),
        P(None, "dp", "tp"),
    )
    out_specs = (
        P("tp", "dp"),
        P(None, "dp", "tp", None, None),
        P(None, "dp", "tp", None),
        P(None, "dp", "tp"),
    )
    return jax.shard_map(
        on_device, mesh=mesh, in_specs=in_specs, out_specs=out_specs, check_vma=False
    )
```

profile of v0, /device:TPU:0, one launch (start us, length us, event | category | flops | bytes accessed | tf_op | source)
XLA Modules:
  0.0 243.8 jit_solution(15858441146114237513)
XLA Ops:
  0.7 32.9 %all-gather = bf16[8,14,1024]{2,1,0:T(8,128)(2,1)S(1)} all-gather(bf16[1,14,1024]{2,1,0:T(8,128)(2,1)} %bitcast.149), channel_id=1, replica_groups=mesh['tp'=8,'dp'=4] {'tp'}, dimensions={0}, use_global_device_ids=true | all-gather | bytes 258048 | tf_op jit(solution)/shard_map/all_gather | solution.py:91
  33.6 1.5 fusion.36
  35.2 1.5 fusion.38
  36.7 1.5 fusion.40
  38.2 2.4 fusion.42
  40.6 14.0 %fusion.93 = (f32[32,512]{1,0:T(8,128)S(1)}, f32[32,512]{1,0:T(8,128)S(1)}, f32[32,512]{1,0:T(8,128)S(1)}, f32[32,512]{1,0:T(8,128)S(1)}) fusion(f32[112,512]{1,0:T(8,128)S(1)} %fusion.36, f32[112,512]{1,0:T(8,128)} %fusion.42, f32[112,512]{1,0:T(8,128)S(1)} %fusion.38, f32[112,512]{1,0:T(8,128)S(1)} %fusion.40), kind=kCustom, calls=%all-reduce-scatter.10 | all-reduce-scatter fusion | flops 262145 | bytes 1180160
  54.6 1.3 collective-permute-start.1
  55.9 3.7 %collective-permute-start.2 = (f32[12,512]{1,0:T(8,128)S(1)}, f32[12,512]{1,0:T(8,128)S(1)}, u32[]{:S(2)}, u32[]{:S(2)}) collective-permute-start(f32[12,512]{1,0:T(8,128)S(1)} %slice.98), channel_id=1, source_target_pairs={{0,1},{1,2},{2,3},{4,5},{5,6},{6,7},{8,9},{9,10},{10,11},{12,13},{... | collective-permute-start | bytes 73736
  59.6 1.9 collective-permute-start
  61.6 1.9 collective-permute-start.3
  63.5 0.1 multiply_reduce_fusion.1
  63.6 1.3 slice_bitcast_fusion.2
  64.9 0.9 fusion.99
  65.8 0.2 convolution_bitcast_fusion
  66.0 0.2 convolution_bitcast_fusion.1
  66.1 1.3 fusion.100
  68.1 5.8 %all-reduce.23 = (f32[112]{0:T(128)S(1)}, f32[112,4]{0,1:T(4,128)S(1)}, f32[112,4]{0,1:T(4,128)S(1)}) all-reduce(f32[112]{0:T(128)S(1)} %multiply_reduce_fusion.1, f32[112,4]{0,1:T(4,128)S(1)} %convolution_bitcast_fusion.1, f32[112,4]{0,1:T(4,128)S(1)} %convolution_bitcast_fusion), channel_id=1, replica_groups=mesh['tp'=8,'dp'=4] {'dp'}, use_global_device_ids=true, to_apply=%region_2.0 | all-reduce | flops 1008 | bytes 8064 | tf_op jit(solution)/shard_map/psum | solution.py:48
  74.1 0.8 maximum_bitcast_fusion.1
  74.9 0.7 slice_bitcast_fusion
  75.6 1.2 dynamic-slice.64
  78.4 0.2 concatenate.1
  78.6 0.2 concatenate.2
  78.8 0.2 concatenate
  79.0 0.2 concatenate.3
  79.4 0.2 fusion.69
  79.7 9.2 %fusion.13 = f32[28,4,1,128]{3,2,1,0:T(1,128)S(1)} fusion(f32[28,4,128,1]{2,3,1,0:T(1,128)S(1)} %bitcast.148, f32[2,28,4,128,128]{4,3,2,1,0:T(8,128)} %param.23, f32[28,4,128]{2,1,0:T(4,128)S(1)} %mul.321, f32[28,4,128]{2,1,0:T(4,128)S(1)} %get-tuple-element.37, f32[28,4]{1,0:T(8,128)S(1)} %copy.41), kind=kOutput, calls=%fused_computation.6 | convolution fusion | flops 27525120 | bytes 7569856 | tf_op jit(solution)/shard_map/bhd,bhde->bhe/dot_general | solution.py:20
  88.9 0.2 fusion.97
  89.1 0.2 multiply_reduce_fusion.3
  89.3 0.1 multiply_convert_fusion.1
  89.4 5.4 %all-gather.1 = bf16[4,28,512]{2,1,0:T(8,128)(2,1)S(1)} all-gather(bf16[1,28,512]{2,1,0:T(8,128)(2,1)S(1)} %reshape.136), channel_id=1, replica_groups=mesh['tp'=8,'dp'=4] {'dp'}, dimensions={0}, use_global_device_ids=true | all-gather | bytes 143360 | tf_op jit(solution)/shard_map/all_gather | solution.py:71
  94.9 0.3 fusion.34
  95.2 43.0 %all-reduce.27 = bf16[112,1024]{1,0:T(8,128)(2,1)S(1)} all-reduce(f32[112,1024]{1,0:T(8,128)S(1)} %fusion.34), channel_id=1, replica_groups=mesh['tp'=8,'dp'=4] {'tp'}, use_global_device_ids=true, to_apply=%region_11.12 | all-reduce | flops 114688 | bytes 688128 | tf_op jit(solution)/shard_map/psum | solution.py:114
  138.2 0.1 multiply_reduce_fusion
  138.4 1.5 fusion.28
  139.9 1.5 fusion.30
  141.4 1.5 fusion.32
  143.0 1.5 fusion.26
  144.5 0.2 fusion.70
  144.7 0.2 fusion.72
  144.8 5.7 %all-reduce.22 = (f32[112]{0:T(128)S(1)}, f32[112,4]{0,1:T(4,128)S(1)}, f32[112,4]{0,1:T(4,128)S(1)}) all-reduce(f32[112]{0:T(128)S(1)} %multiply_reduce_fusion, f32[112,4]{0,1:T(4,128)S(1)} %fusion.72, f32[112,4]{0,1:T(4,128)S(1)} %fusion.70), channel_id=1, replica_groups=mesh['tp'=8,'dp'=4] {'dp'}, use_global_device_ids=true, to_apply=%region_14.15 | all-reduce | flops 1008 | bytes 8064 | tf_op jit(solution)/shard_map/psum | solution.py:48
  150.9 14.6 %fusion.92 = (f32[32,512]{1,0:T(8,128)S(1)}, f32[32,512]{1,0:T(8,128)S(1)}, f32[32,512]{1,0:T(8,128)S(1)}, f32[32,512]{1,0:T(8,128)S(1)}) fusion(f32[112,512]{1,0:T(8,128)S(1)} %fusion.26, f32[112,512]{1,0:T(8,128)S(1)} %fusion.32, f32[112,512]{1,0:T(8,128)S(1)} %fusion.28, f32[112,512]{1,0:T(8,128)S(1)} %fusion.30), kind=kCustom, calls=%all-reduce-scatter.9 | all-reduce-scatter fusion | flops 262145 | bytes 1180160
  165.5 1.3 collective-permute-start.5
  166.8 3.8 %collective-permute-start.6 = (f32[12,512]{1,0:T(8,128)S(1)}, f32[12,512]{1,0:T(8,128)S(1)}, u32[]{:S(2)}, u32[]{:S(2)}) collective-permute-start(f32[12,512]{1,0:T(8,128)S(1)} %slice.102), channel_id=1, source_target_pairs={{0,1},{1,2},{2,3},{4,5},{5,6},{6,7},{8,9},{9,10},{10,11},{12,13},{... | collective-permute-start | bytes 73736
  170.6 1.9 collective-permute-start.4
  172.6 2.1 collective-permute-start.7
  174.7 0.6 pad_maximum_fusion.2
  175.5 0.2 concatenate.5
  175.7 0.2 concatenate.6
  175.9 0.2 concatenate.4
  176.1 0.2 concatenate.7
  176.6 0.2 fusion.66
  176.8 14.1 %multiply_add_fusion.1 = (f32[1,28,4,128,128]{4,3,2,1,0:T(8,128)}, f32[1,28,4,128,128]{4,3,2,1,0:T(8,128)}) fusion(f32[2,28,4,128,128]{4,3,2,1,0:T(8,128)} %param.23, f32[28,4,128]{2,1,0:T(4,128)S(1)} %mul.321, f32[28,4,128]{2,1,0:T(4,128)S(1)} %get-tuple-element.37, f32[28,4]{1,0:T(8,128)S(1)} %copy.41, f32[28,4,128]{2,1,0:T(4,128)S(1)} %mul.347, ...), kind=kLoop, calls=%fused_computation.8 | loop fusion | flops 11010048 | bytes 29590400 | tf_op jit(solution)/shard_map/add | solution.py:16
  190.9 6.9 %fusion.10 = f32[28,4,1,128]{3,2,1,0:T(1,128)S(1)} fusion(f32[28,4,128,1]{2,3,1,0:T(1,128)S(1)} %bitcast.147, f32[2,28,4,128,128]{4,3,2,1,0:T(8,128)S(1)} %bitcast.144, f32[28,4,128]{2,1,0:T(4,128)S(1)} %mul.347, f32[28,4,128]{2,1,0:T(4,128)S(1)} %get-tuple-element.33, f32[28,4]{1,0:T(8,128)S(1)} %copy.44), kind=kOutput, calls=%fused_computation.3 | convolution fusion | flops 27525120 | bytes 7585792 | tf_op jit(solution)/shard_map/bhd,bhde->bhe/dot_general | solution.py:20
  197.9 0.2 fusion.96
  198.1 0.2 multiply_reduce_fusion.2
  198.4 5.4 %all-gather.2 = bf16[4,28,512]{2,1,0:T(8,128)(2,1)S(1)} all-gather(bf16[1,28,512]{2,1,0:T(8,128)(2,1)S(1)} %reshape.138), channel_id=1, replica_groups=mesh['tp'=8,'dp'=4] {'dp'}, dimensions={0}, use_global_device_ids=true | all-gather | bytes 143360 | tf_op jit(solution)/shard_map/all_gather | solution.py:71
  203.9 1.5 convolution_convert_fusion
  205.4 21.2 %fusion.8 = bf16[16,1024]{1,0:T(8,128)(2,1)S(1)} fusion(bf16[112,1024]{1,0:T(8,128)(2,1)S(1)} %convolution_convert_fusion), kind=kCustom, calls=%all-reduce-scatter.8 | all-reduce-scatter fusion | flops 131073 | bytes 262656
  226.6 2.1 collective-permute-start.8
  228.7 0.2 multiply_add_fusion.3
  228.9 13.4 %pad_maximum_fusion = f32[2,28,4,128,128]{4,3,2,1,0:T(8,128)} fusion(f32[1,28,4,128,128]{4,3,2,1,0:T(8,128)} %get-tuple-element.39, f32[1,28,4,128,128]{4,3,2,1,0:T(8,128)} %get-tuple-element.38), kind=kLoop, calls=%fused_computation | loop fusion | flops 3670016 | bytes 29360128 | tf_op jit(solution)/shard_map/stack | solution.py:119
  242.3 0.7 pad_maximum_fusion.1
  242.9 0.2 concatenate.8
  243.1 0.6 constant_dynamic-slice_fusion
  (73 shorter events, 1.8 us)
Async XLA Ops:
  0.6 64.3 %copy-start.2 = (bf16[2,1024,32]{1,2,0:T(8,128)(2,1)S(1)}, bf16[2,1024,32]{1,2,0:T(8,128)(2,1)}, u32[]{:S(2)}) copy-start(bf16[2,1024,32]{1,2,0:T(8,128)(2,1)} %param.18) | copy-start | bytes 393220
  0.6 78.8 %copy-start.1 = (f32[2,28,4,128]{3,2,1,0:T(4,128)S(1)}, f32[2,28,4,128]{3,2,1,0:T(4,128)}, u32[]{:S(2)}) copy-start(f32[2,28,4,128]{3,2,1,0:T(4,128)} %param.24) | copy-start | bytes 344068
  38.2 56.7 %copy-start = (bf16[2,512,1024]{2,1,0:T(8,128)(2,1)S(1)}, bf16[2,512,1024]{2,1,0:T(8,128)(2,1)}, u32[]{:S(2)}) copy-start(bf16[2,512,1024]{2,1,0:T(8,128)(2,1)} %param.22) | copy-start | bytes 6291460
  54.6 23.8 %collective-permute-start.1 = (f32[12,512]{1,0:T(8,128)S(1)}, f32[12,512]{1,0:T(8,128)S(1)}, u32[]{:S(2)}, u32[]{:S(2)}) collective-permute-start(f32[12,512]{1,0:T(8,128)S(1)} %slice.97), channel_id=1, source_target_pairs={{0,1},{1,2},{2,3},{4,5},{5,6},{6,7},{8,9},{9,10},{10,11},{12,13},{... | collective-permute-start | bytes 73736
  55.9 22.6 %collective-permute-start.2 = (f32[12,512]{1,0:T(8,128)S(1)}, f32[12,512]{1,0:T(8,128)S(1)}, u32[]{:S(2)}, u32[]{:S(2)}) collective-permute-start(f32[12,512]{1,0:T(8,128)S(1)} %slice.98), channel_id=1, source_target_pairs={{0,1},{1,2},{2,3},{4,5},{5,6},{6,7},{8,9},{9,10},{10,11},{12,13},{... | collective-permute-start | bytes 73736
  59.6 19.2 %collective-permute-start = (f32[12,512]{1,0:T(8,128)S(1)}, f32[12,512]{1,0:T(8,128)S(1)}, u32[]{:S(2)}, u32[]{:S(2)}) collective-permute-start(f32[12,512]{1,0:T(8,128)S(1)} %slice.96), channel_id=1, source_target_pairs={{0,1},{1,2},{2,3},{4,5},{5,6},{6,7},{8,9},{9,10},{10,11},{12,13},{... | collective-permute-start | bytes 73736
  61.6 17.4 %collective-permute-start.3 = (f32[12,512]{1,0:T(8,128)S(1)}, f32[12,512]{1,0:T(8,128)S(1)}, u32[]{:S(2)}, u32[]{:S(2)}) collective-permute-start(f32[12,512]{1,0:T(8,128)S(1)} %slice.99), channel_id=1, source_target_pairs={{0,1},{1,2},{2,3},{4,5},{5,6},{6,7},{8,9},{9,10},{10,11},{12,13},{... | collective-permute-start | bytes 73736
  79.7 71.0 %copy-start.3 = (f32[2,28,4]{1,2,0:T(4,128)S(1)}, f32[2,28,4]{1,2,0:T(4,128)}, u32[]{:S(2)}) copy-start(f32[2,28,4]{1,2,0:T(4,128)} %param.25) | copy-start | bytes 2692
  79.7 71.0 %copy-start.4 = (f32[4]{0:T(128)S(1)}, f32[4]{0:T(128)}, u32[]{:S(2)}) copy-start(f32[4]{0:T(128)} %get-tuple-element.52) | copy-start | bytes 52
  165.5 10.0 %collective-permute-start.5 = (f32[12,512]{1,0:T(8,128)S(1)}, f32[12,512]{1,0:T(8,128)S(1)}, u32[]{:S(2)}, u32[]{:S(2)}) collective-permute-start(f32[12,512]{1,0:T(8,128)S(1)} %slice.101), channel_id=1, source_target_pairs={{0,1},{1,2},{2,3},{4,5},{5,6},{6,7},{8,9},{9,10},{10,11},{12,13},{... | collective-permute-start | bytes 73736
  166.8 8.9 %collective-permute-start.6 = (f32[12,512]{1,0:T(8,128)S(1)}, f32[12,512]{1,0:T(8,128)S(1)}, u32[]{:S(2)}, u32[]{:S(2)}) collective-permute-start(f32[12,512]{1,0:T(8,128)S(1)} %slice.102), channel_id=1, source_target_pairs={{0,1},{1,2},{2,3},{4,5},{5,6},{6,7},{8,9},{9,10},{10,11},{12,13},{... | collective-permute-start | bytes 73736
  170.6 5.2 %collective-permute-start.4 = (f32[12,512]{1,0:T(8,128)S(1)}, f32[12,512]{1,0:T(8,128)S(1)}, u32[]{:S(2)}, u32[]{:S(2)}) collective-permute-start(f32[12,512]{1,0:T(8,128)S(1)} %slice.100), channel_id=1, source_target_pairs={{0,1},{1,2},{2,3},{4,5},{5,6},{6,7},{8,9},{9,10},{10,11},{12,13},{... | collective-permute-start | bytes 73736
  172.6 3.5 %collective-permute-start.7 = (f32[12,512]{1,0:T(8,128)S(1)}, f32[12,512]{1,0:T(8,128)S(1)}, u32[]{:S(2)}, u32[]{:S(2)}) collective-permute-start(f32[12,512]{1,0:T(8,128)S(1)} %slice.103), channel_id=1, source_target_pairs={{0,1},{1,2},{2,3},{4,5},{5,6},{6,7},{8,9},{9,10},{10,11},{12,13},{... | collective-permute-start | bytes 73736
  176.5 14.4 %slice-start = ((s8[14680064]{0:T(1024)(128)(4,1)}), s8[2097152]{0:T(1024)(128)(4,1)S(1)}, s32[]{:S(2)}) async-start(s8[14680064]{0:T(1024)(128)(4,1)} %bitcast.143), calls=%async_computation | async-start | bytes 4194304
  176.8 14.1 %slice-start.1 = ((s8[14680064]{0:T(1024)(128)(4,1)}), s8[4194304]{0:T(1024)(128)(4,1)S(1)}, s32[]{:S(2)}) async-start(s8[14680064]{0:T(1024)(128)(4,1)} %bitcast.143), calls=%async_computation.1 | async-start | bytes 8388608
  176.8 14.1 %slice-start.2 = ((s8[14680064]{0:T(1024)(128)(4,1)}), s8[4194304]{0:T(1024)(128)(4,1)S(1)}, s32[]{:S(2)}) async-start(s8[14680064]{0:T(1024)(128)(4,1)} %bitcast.143), calls=%async_computation.2 | async-start | bytes 8388608
  176.8 14.1 %slice-start.3 = ((s8[14680064]{0:T(1024)(128)(4,1)}), s8[4194304]{0:T(1024)(128)(4,1)S(1)}, s32[]{:S(2)}) async-start(s8[14680064]{0:T(1024)(128)(4,1)} %bitcast.143), calls=%async_computation.3 | async-start | bytes 8388608
  226.6 16.3 %collective-permute-start.8 = (bf16[14,1024]{1,0:T(8,128)(2,1)S(1)}, bf16[14,1024]{1,0:T(8,128)(2,1)S(1)}, u32[]{:S(2)}, u32[]{:S(2)}) collective-permute-start(bf16[14,1024]{1,0:T(8,128)(2,1)S(1)} %slice.104), channel_id=1, source_target_pairs={{0,4},{4,8},{8,12},{12,16},{16,20},{20,24},{24,28},{1,5},{5,9},{9,... | collective-permute-start | bytes 86024
where the time goes:
time: 245 us; the launch traced here: 244 us
  blocking collectives  148 us (60%)
  other arithmetic  31.9 us (13%)
  matrix products  31.7 us (13%)
  starting transfers between devices  20 us (8%)
  local copies, waits for them, and re-layouts  8.64 us (4%)
  between operations  3.34 us (1%)
    unnamed x3, blocking collectives  49.8 us
    psum x1, blocking collectives, on_device(): current = lax.psum(out_partial, 'tp').astype(jnp.bfloat16)  43 us
    all_gather x1, blocking collectives, on_device(): current = lax.all_gather(tokens, 'tp', axis=0, tiled=True)  32.9 us
    unnamed x9, starting transfers between devices  20 us
    dot_general x2, matrix products, cell_update(): jnp.einsum('bhd,bhde->bhe', queries, matrix_new, precision=lax.Precision....  16.1 us
    add x1, other arithmetic, cell_update(): decays[..., None, None] * matrix  14.1 us
    another operation x1, other arithmetic, on_device(): jnp.stack(matrix_list)  13.4 us
    psum x2, blocking collectives, mix_block(): totals = lax.psum(squares, 'dp')  11.6 us
  transfers between devices with their start and end apart: 9, of which 0 were waited for; matrix products, arithmetic and copies ran while one was open for 10% of the time, Pallas kernels for 0%

commit v1 on v0

--- a/solution.py
+++ b/solution.py
@@ -88,7 +88,12 @@
     mem_norm,
     mem_max,
 ):
-    current = lax.all_gather(tokens, "tp", axis=0, tiled=True)
+    ring = [tokens]
+    for hop in range(7):
+        ring.append(lax.ppermute(ring[-1], "tp", [(dev, (dev + 1) % 8) for dev in range(8)]))
+    current = jnp.roll(
+        jnp.concatenate(ring[::-1], axis=0), (lax.axis_index("tp") + 1) * ring[0].shape[0], axis=0
+    )
     matrix_list, norm_list, max_list = ([], [], [])
     block_total = w_query.shape[0]
     result = current

time: 245 us -> 254 us (1.037)
  waiting for transfers between devices: 0.02 us -> 36.3 us
  blocking collectives: 148 us -> 114 us
  local copies, waits for them, and re-layouts: 8.64 us -> 13.2 us
  starting transfers between devices: 20 us -> 23 us
    ppermute x0 -> x7, waiting for transfers between devices: none -> 36.2 us  [on_device(): lax.ppermute(ring[-1], 'tp', [(dev, (dev + 1) % 8) for dev in range(8)])]
    all_gather x1 -> x0, blocking collectives: 32.9 us -> none  [on_device(): current = lax.all_gather(tokens, 'tp', axis=0, tiled=True)]
    concatenate x0 -> x1, local copies, waits for them, and re-layouts: none -> 3.13 us  [on_device(): jnp.roll(jnp.concatenate(ring[::-1], axis=0), (lax.axis_index('tp') + 1)...]
    ppermute x0 -> x7, starting transfers between devices: none -> 3.04 us  [on_device(): lax.ppermute(ring[-1], 'tp', [(dev, (dev + 1) % 8) for dev in range(8)])]
    unnamed x44 -> x45, local copies, waits for them, and re-layouts: 5.11 us -> 5.03 us
  transfers between devices with their start and end apart: 9 -> 16, of which waited for: 0 -> 7; matrix products, arithmetic and copies ran while one was open for 10% -> 9% of each run, Pallas kernels for 0% -> 0%
where the time goes in v1:
time: 254 us; the launch traced here: 253 us
  blocking collectives  114 us (45%)
  waiting for transfers between devices  36.3 us (14%)
  matrix products  32.4 us (13%)
  other arithmetic  31.3 us (12%)
  starting transfers between devices  23 us (9%)
  local copies, waits for them, and re-layouts  13.2 us (5%)
  between operations  3.34 us (1%)
    unnamed x3, blocking collectives  49.3 us
    psum x1, blocking collectives, on_device(): current = lax.psum(out_partial, 'tp').astype(jnp.bfloat16)  42.1 us
    ppermute x7, waiting for transfers between devices, on_device(): lax.ppermute(ring[-1], 'tp', [(dev, (dev + 1) % 8) for dev in range(8)])  36.2 us
    unnamed x9, starting transfers between devices  20 us
    dot_general x2, matrix products, cell_update(): jnp.einsum('bhd,bhde->bhe', queries, matrix_new, precision=lax.Precision....  16.1 us
    add x1, other arithmetic, cell_update(): decays[..., None, None] * matrix  14.1 us
    another operation x1, other arithmetic, on_device(): jnp.stack(matrix_list)  13.4 us
    psum x2, blocking collectives, mix_block(): totals = lax.psum(squares, 'dp')  11.6 us
  transfers between devices with their start and end apart: 16, of which 7 were waited for; matrix products, arithmetic and copies ran while one was open for 9% of the time, Pallas kernels for 0%

profile of v1, /device:TPU:0, one launch (start us, length us, event | category | flops | bytes accessed | tf_op | source)
XLA Modules:
  0.0 253.3 jit_solution(12684498387717795986)
XLA Ops:
  0.7 3.0 %collective-permute-start = (bf16[14,1024]{1,0:T(8,128)(2,1)}, bf16[14,1024]{1,0:T(8,128)(2,1)S(1)}, u32[]{:S(2)}, u32[]{:S(2)}) collective-permute-start(bf16[14,1024]{1,0:T(8,128)(2,1)} %param.13), channel_id=1, source_target_pairs={{0,4},{4,8},{8,12},{12,16},{16,20},{20,24},{24,28},{28,0},{1,5},{5... | collective-permute-start | bytes 86024 | tf_op jit(solution)/shard_map/ppermute | solution.py:93
  3.7 5.1 %collective-permute-done = bf16[14,1024]{1,0:T(8,128)(2,1)S(1)} collective-permute-done((bf16[14,1024]{1,0:T(8,128)(2,1)}, bf16[14,1024]{1,0:T(8,128)(2,1)S(1)}, u32[]{:S(2)}, u32[]{:S(2)}) %collective-permute-start) | collective-permute-done | bytes 28704 | tf_op jit(solution)/shard_map/ppermute | solution.py:93
  8.8 6.6 %collective-permute-done.1 = bf16[14,1024]{1,0:T(8,128)(2,1)S(1)} collective-permute-done((bf16[14,1024]{1,0:T(8,128)(2,1)S(1)}, bf16[14,1024]{1,0:T(8,128)(2,1)S(1)}, u32[]{:S(2)}, u32[]{:S(2)}) %collective-permute-start.1) | collective-permute-done | bytes 28704 | tf_op jit(solution)/shard_map/ppermute | solution.py:93
  15.4 6.6 %collective-permute-done.2 = bf16[14,1024]{1,0:T(8,128)(2,1)S(1)} collective-permute-done((bf16[14,1024]{1,0:T(8,128)(2,1)S(1)}, bf16[14,1024]{1,0:T(8,128)(2,1)S(1)}, u32[]{:S(2)}, u32[]{:S(2)}) %collective-permute-start.2) | collective-permute-done | bytes 28704 | tf_op jit(solution)/shard_map/ppermute | solution.py:93
  22.0 0.9 fusion.110
  22.9 5.7 %collective-permute-done.3 = bf16[14,1024]{1,0:T(8,128)(2,1)S(1)} collective-permute-done((bf16[14,1024]{1,0:T(8,128)(2,1)S(1)}, bf16[14,1024]{1,0:T(8,128)(2,1)S(1)}, u32[]{:S(2)}, u32[]{:S(2)}) %collective-permute-start.3) | collective-permute-done | bytes 28704 | tf_op jit(solution)/shard_map/ppermute | solution.py:93
  28.7 0.9 fusion.111
  29.5 6.1 %collective-permute-done.4 = bf16[14,1024]{1,0:T(8,128)(2,1)S(1)} collective-permute-done((bf16[14,1024]{1,0:T(8,128)(2,1)S(1)}, bf16[14,1024]{1,0:T(8,128)(2,1)S(1)}, u32[]{:S(2)}, u32[]{:S(2)}) %collective-permute-start.4) | collective-permute-done | bytes 28704 | tf_op jit(solution)/shard_map/ppermute | solution.py:93
  35.6 1.3 slice_bitcast_fusion
  36.9 5.3 %collective-permute-done.5 = bf16[14,1024]{1,0:T(8,128)(2,1)S(1)} collective-permute-done((bf16[14,1024]{1,0:T(8,128)(2,1)S(1)}, bf16[14,1024]{1,0:T(8,128)(2,1)S(1)}, u32[]{:S(2)}, u32[]{:S(2)}) %collective-permute-start.5) | collective-permute-done | bytes 28704 | tf_op jit(solution)/shard_map/ppermute | solution.py:93
  42.2 1.3 slice_bitcast_fusion.2
  43.6 1.2 dynamic-slice.64
  45.4 1.3 fusion.112
  48.1 0.8 collective-permute-done.6
  48.8 3.1 %concatenate.6 = bf16[224,1024]{1,0:T(8,128)(2,1)S(1)} concatenate(bf16[14,1024]{1,0:T(8,128)(2,1)S(1)} %collective-permute-done.6, bf16[14,1024]{1,0:T(8,128)(2,1)S(1)} %collective-permute-done.5, bf16[14,1024]{1,0:T(8,128)(2,1)S(1)} %collective-permute-done.4, bf16[14,1024]{1,0:T(8,128)(2,1)S(1)} %collective-permute-done.3, bf16[14,1024]{1,0:T(8,128)(2,1)S(1)} %collective-permute-done.2, ...), dimensions={0} | concatenate | bytes 917504 | tf_op jit(solution)/shard_map/jit(_roll_dynamic)/concatenate | solution.py:94
  52.1 0.2 fusion.69
  52.3 0.2 fusion.67
  52.5 1.5 fusion.40
  54.0 1.5 fusion.38
  55.6 2.4 fusion.36
  58.0 2.2 fusion.42
  60.2 13.9 %fusion.105 = (f32[32,512]{1,0:T(8,128)S(1)}, f32[32,512]{1,0:T(8,128)S(1)}, f32[32,512]{1,0:T(8,128)S(1)}, f32[32,512]{1,0:T(8,128)S(1)}) fusion(f32[112,512]{1,0:T(8,128)} %fusion.36, f32[112,512]{1,0:T(8,128)} %fusion.42, f32[112,512]{1,0:T(8,128)S(1)} %fusion.38, f32[112,512]{1,0:T(8,128)S(1)} %fusion.40), kind=kCustom, calls=%all-reduce-scatter.10 | all-reduce-scatter fusion | flops 262145 | bytes 1180160
  74.2 1.3 collective-permute-start.8
  75.5 3.7 %collective-permute-start.9 = (f32[12,512]{1,0:T(8,128)S(1)}, f32[12,512]{1,0:T(8,128)S(1)}, u32[]{:S(2)}, u32[]{:S(2)}) collective-permute-start(f32[12,512]{1,0:T(8,128)S(1)} %slice.98), channel_id=1, source_target_pairs={{0,1},{1,2},{2,3},{4,5},{5,6},{6,7},{8,9},{9,10},{10,11},{12,13},{... | collective-permute-start | bytes 73736
  79.2 1.9 collective-permute-start.7
  81.1 1.9 collective-permute-start.10
  83.0 5.8 %all-reduce.23 = (f32[112]{0:T(128)S(1)}, f32[112,4]{0,1:T(4,128)S(1)}, f32[112,4]{0,1:T(4,128)S(1)}) all-reduce(f32[112]{0:T(128)S(1)} %multiply_reduce_fusion.1, f32[112,4]{0,1:T(4,128)S(1)} %fusion.69, f32[112,4]{0,1:T(4,128)S(1)} %fusion.67), channel_id=1, replica_groups=mesh['tp'=8,'dp'=4] {'dp'}, use_global_device_ids=true, to_apply=%region_2.3 | all-reduce | flops 1008 | bytes 8064 | tf_op jit(solution)/shard_map/psum | solution.py:48
  89.3 0.2 concatenate.8
  89.5 0.2 concatenate.9
  89.7 0.2 concatenate.7
  89.9 0.2 concatenate.10
  90.4 0.2 fusion.77
  90.6 9.2 %fusion.13 = f32[28,4,1,128]{3,2,1,0:T(1,128)S(1)} fusion(f32[28,4,128,1]{2,3,1,0:T(1,128)S(1)} %bitcast.137, f32[2,28,4,128,128]{4,3,2,1,0:T(8,128)} %param.23, f32[28,4,128]{2,1,0:T(4,128)S(1)} %mul.325, f32[28,4,128]{2,1,0:T(4,128)S(1)} %get-tuple-element.37, f32[28,4]{1,0:T(8,128)S(1)} %copy.41), kind=kOutput, calls=%fused_computation.6 | convolution fusion | flops 27525120 | bytes 7569856 | tf_op jit(solution)/shard_map/bhd,bhde->bhe/dot_general | solution.py:20
  99.8 0.2 fusion.109
  100.4 5.4 %all-gather = bf16[4,28,512]{2,1,0:T(8,128)(2,1)S(1)} all-gather(bf16[1,28,512]{2,1,0:T(8,128)(2,1)S(1)} %reshape.134), channel_id=1, replica_groups=mesh['tp'=8,'dp'=4] {'dp'}, dimensions={0}, use_global_device_ids=true | all-gather | bytes 143360 | tf_op jit(solution)/shard_map/all_gather | solution.py:71
  105.8 0.3 fusion.34
  106.1 42.1 %all-reduce.27 = bf16[112,1024]{1,0:T(8,128)(2,1)S(1)} all-reduce(f32[112,1024]{1,0:T(8,128)S(1)} %fusion.34), channel_id=1, replica_groups=mesh['tp'=8,'dp'=4] {'tp'}, use_global_device_ids=true, to_apply=%region_11.12 | all-reduce | flops 114688 | bytes 688128 | tf_op jit(solution)/shard_map/psum | solution.py:119
  148.4 1.5 fusion.28
  149.9 1.5 fusion.30
  151.4 1.5 fusion.32
  153.0 1.5 fusion.26
  154.7 0.2 fusion.80
  154.8 5.7 %all-reduce.22 = (f32[112]{0:T(128)S(1)}, f32[112,4]{0,1:T(4,128)S(1)}, f32[112,4]{0,1:T(4,128)S(1)}) all-reduce(f32[112]{0:T(128)S(1)} %multiply_reduce_fusion, f32[112,4]{0,1:T(4,128)S(1)} %fusion.80, f32[112,4]{0,1:T(4,128)S(1)} %fusion.78), channel_id=1, replica_groups=mesh['tp'=8,'dp'=4] {'dp'}, use_global_device_ids=true, to_apply=%region_14.15 | all-reduce | flops 1008 | bytes 8064 | tf_op jit(solution)/shard_map/psum | solution.py:48
  160.8 14.6 %fusion.104 = (f32[32,512]{1,0:T(8,128)S(1)}, f32[32,512]{1,0:T(8,128)S(1)}, f32[32,512]{1,0:T(8,128)S(1)}, f32[32,512]{1,0:T(8,128)S(1)}) fusion(f32[112,512]{1,0:T(8,128)S(1)} %fusion.26, f32[112,512]{1,0:T(8,128)S(1)} %fusion.32, f32[112,512]{1,0:T(8,128)S(1)} %fusion.28, f32[112,512]{1,0:T(8,128)S(1)} %fusion.30), kind=kCustom, calls=%all-reduce-scatter.9 | all-reduce-scatter fusion | flops 262145 | bytes 1180160
  175.5 1.3 collective-permute-start.12
  176.8 3.8 %collective-permute-start.13 = (f32[12,512]{1,0:T(8,128)S(1)}, f32[12,512]{1,0:T(8,128)S(1)}, u32[]{:S(2)}, u32[]{:S(2)}) collective-permute-start(f32[12,512]{1,0:T(8,128)S(1)} %slice.102), channel_id=1, source_target_pairs={{0,1},{1,2},{2,3},{4,5},{5,6},{6,7},{8,9},{9,10},{10,11},{12,13},{... | collective-permute-start | bytes 73736
  180.6 1.9 collective-permute-start.11
  182.5 2.1 collective-permute-start.14
  184.7 0.6 pad_maximum_fusion.2
  185.7 0.2 concatenate.13
  185.9 0.2 concatenate.11
  186.1 0.2 concatenate.14
  186.6 0.2 fusion.74
  186.8 14.1 %multiply_add_fusion.1 = (f32[1,28,4,128,128]{4,3,2,1,0:T(8,128)}, f32[1,28,4,128,128]{4,3,2,1,0:T(8,128)}) fusion(f32[2,28,4,128,128]{4,3,2,1,0:T(8,128)} %param.23, f32[28,4,128]{2,1,0:T(4,128)S(1)} %mul.325, f32[28,4,128]{2,1,0:T(4,128)S(1)} %get-tuple-element.37, f32[28,4]{1,0:T(8,128)S(1)} %copy.41, f32[28,4,128]{2,1,0:T(4,128)S(1)} %mul.351, ...), kind=kLoop, calls=%fused_computation.8 | loop fusion | flops 11010048 | bytes 29590400 | tf_op jit(solution)/shard_map/add | solution.py:16
  200.9 6.9 %fusion.10 = f32[28,4,1,128]{3,2,1,0:T(1,128)S(1)} fusion(f32[28,4,128,1]{2,3,1,0:T(1,128)S(1)} %bitcast.136, f32[2,28,4,128,128]{4,3,2,1,0:T(8,128)S(1)} %bitcast.133, f32[28,4,128]{2,1,0:T(4,128)S(1)} %mul.351, f32[28,4,128]{2,1,0:T(4,128)S(1)} %get-tuple-element.33, f32[28,4]{1,0:T(8,128)S(1)} %copy.44), kind=kOutput, calls=%fused_computation.3 | convolution fusion | flops 27525120 | bytes 7585792 | tf_op jit(solution)/shard_map/bhd,bhde->bhe/dot_general | solution.py:20
  207.9 0.2 fusion.108
  208.4 5.4 %all-gather.1 = bf16[4,28,512]{2,1,0:T(8,128)(2,1)S(1)} all-gather(bf16[1,28,512]{2,1,0:T(8,128)(2,1)S(1)} %reshape.136), channel_id=1, replica_groups=mesh['tp'=8,'dp'=4] {'dp'}, dimensions={0}, use_global_device_ids=true | all-gather | bytes 143360 | tf_op jit(solution)/shard_map/all_gather | solution.py:71
  213.9 1.5 convolution_convert_fusion
  215.4 20.8 %fusion.8 = bf16[16,1024]{1,0:T(8,128)(2,1)S(1)} fusion(bf16[112,1024]{1,0:T(8,128)(2,1)S(1)} %convolution_convert_fusion), kind=kCustom, calls=%all-reduce-scatter.8 | all-reduce-scatter fusion | flops 131073 | bytes 262656
  236.2 2.0 collective-permute-start.15
  238.3 0.2 multiply_add_fusion.3
  238.4 13.4 %pad_maximum_fusion = f32[2,28,4,128,128]{4,3,2,1,0:T(8,128)} fusion(f32[1,28,4,128,128]{4,3,2,1,0:T(8,128)} %get-tuple-element.39, f32[1,28,4,128,128]{4,3,2,1,0:T(8,128)} %get-tuple-element.38), kind=kLoop, calls=%fused_computation | loop fusion | flops 3670016 | bytes 29360128 | tf_op jit(solution)/shard_map/stack | solution.py:124
  251.8 0.7 pad_maximum_fusion.1
  252.7 0.6 constant_dynamic-slice_fusion
  (88 shorter events, 3.1 us)
Async XLA Ops:
  0.6 88.3 %copy-start.3 = (f32[2,28,4]{1,2,0:T(4,128)S(1)}, f32[2,28,4]{1,2,0:T(4,128)}, u32[]{:S(2)}) copy-start(f32[2,28,4]{1,2,0:T(4,128)} %param.25) | copy-start | bytes 2692
  0.6 89.7 %copy-start.1 = (f32[2,28,4,128]{3,2,1,0:T(4,128)S(1)}, f32[2,28,4,128]{3,2,1,0:T(4,128)}, u32[]{:S(2)}) copy-start(f32[2,28,4,128]{3,2,1,0:T(4,128)} %param.24) | copy-start | bytes 344068
  0.7 8.2 %collective-permute-start = (bf16[14,1024]{1,0:T(8,128)(2,1)}, bf16[14,1024]{1,0:T(8,128)(2,1)S(1)}, u32[]{:S(2)}, u32[]{:S(2)}) collective-permute-start(bf16[14,1024]{1,0:T(8,128)(2,1)} %param.13), channel_id=1, source_target_pairs={{0,4},{4,8},{8,12},{12,16},{16,20},{20,24},{24,28},{28,0},{1,5},{5... | collective-permute-start | bytes 86024 | tf_op jit(solution)/shard_map/ppermute | solution.py:93
  8.8 6.6 %collective-permute-start.1 = (bf16[14,1024]{1,0:T(8,128)(2,1)S(1)}, bf16[14,1024]{1,0:T(8,128)(2,1)S(1)}, u32[]{:S(2)}, u32[]{:S(2)}) collective-permute-start(bf16[14,1024]{1,0:T(8,128)(2,1)S(1)} %collective-permute-done), channel_id=1, source_target_pairs={{0,4},{4,8},{8,12},{12,16},{16,20},{20,24},{24,28},{28,0},{1,5},{5... | collective-permute-start | bytes 86024 | tf_op jit(solution)/shard_map/ppermute | solution.py:93
  15.4 6.6 %collective-permute-start.2 = (bf16[14,1024]{1,0:T(8,128)(2,1)S(1)}, bf16[14,1024]{1,0:T(8,128)(2,1)S(1)}, u32[]{:S(2)}, u32[]{:S(2)}) collective-permute-start(bf16[14,1024]{1,0:T(8,128)(2,1)S(1)} %collective-permute-done.1), channel_id=1, source_target_pairs={{0,4},{4,8},{8,12},{12,16},{16,20},{20,24},{24,28},{28,0},{1,5},{5... | collective-permute-start | bytes 86024 | tf_op jit(solution)/shard_map/ppermute | solution.py:93
  22.0 6.6 %collective-permute-start.3 = (bf16[14,1024]{1,0:T(8,128)(2,1)S(1)}, bf16[14,1024]{1,0:T(8,128)(2,1)S(1)}, u32[]{:S(2)}, u32[]{:S(2)}) collective-permute-start(bf16[14,1024]{1,0:T(8,128)(2,1)S(1)} %collective-permute-done.2), channel_id=1, source_target_pairs={{0,4},{4,8},{8,12},{12,16},{16,20},{20,24},{24,28},{28,0},{1,5},{5... | collective-permute-start | bytes 86024 | tf_op jit(solution)/shard_map/ppermute | solution.py:93
  28.7 7.0 %collective-permute-start.4 = (bf16[14,1024]{1,0:T(8,128)(2,1)S(1)}, bf16[14,1024]{1,0:T(8,128)(2,1)S(1)}, u32[]{:S(2)}, u32[]{:S(2)}) collective-permute-start(bf16[14,1024]{1,0:T(8,128)(2,1)S(1)} %collective-permute-done.3), channel_id=1, source_target_pairs={{0,4},{4,8},{8,12},{12,16},{16,20},{20,24},{24,28},{28,0},{1,5},{5... | collective-permute-start | bytes 86024 | tf_op jit(solution)/shard_map/ppermute | solution.py:93
  35.6 6.6 %collective-permute-start.5 = (bf16[14,1024]{1,0:T(8,128)(2,1)S(1)}, bf16[14,1024]{1,0:T(8,128)(2,1)S(1)}, u32[]{:S(2)}, u32[]{:S(2)}) collective-permute-start(bf16[14,1024]{1,0:T(8,128)(2,1)S(1)} %collective-permute-done.4), channel_id=1, source_target_pairs={{0,4},{4,8},{8,12},{12,16},{16,20},{20,24},{24,28},{28,0},{1,5},{5... | collective-permute-start | bytes 86024 | tf_op jit(solution)/shard_map/ppermute | solution.py:93
  42.2 6.6 %collective-permute-start.6 = (bf16[14,1024]{1,0:T(8,128)(2,1)S(1)}, bf16[14,1024]{1,0:T(8,128)(2,1)S(1)}, u32[]{:S(2)}, u32[]{:S(2)}) collective-permute-start(bf16[14,1024]{1,0:T(8,128)(2,1)S(1)} %collective-permute-done.5), channel_id=1, source_target_pairs={{0,4},{4,8},{8,12},{12,16},{16,20},{20,24},{24,28},{28,0},{1,5},{5... | collective-permute-start | bytes 86024 | tf_op jit(solution)/shard_map/ppermute | solution.py:93
  55.6 50.2 %copy-start = (bf16[2,512,1024]{2,1,0:T(8,128)(2,1)S(1)}, bf16[2,512,1024]{2,1,0:T(8,128)(2,1)}, u32[]{:S(2)}) copy-start(bf16[2,512,1024]{2,1,0:T(8,128)(2,1)} %param.22) | copy-start | bytes 6291460
  74.2 15.2 %collective-permute-start.8 = (f32[12,512]{1,0:T(8,128)S(1)}, f32[12,512]{1,0:T(8,128)S(1)}, u32[]{:S(2)}, u32[]{:S(2)}) collective-permute-start(f32[12,512]{1,0:T(8,128)S(1)} %slice.97), channel_id=1, source_target_pairs={{0,1},{1,2},{2,3},{4,5},{5,6},{6,7},{8,9},{9,10},{10,11},{12,13},{... | collective-permute-start | bytes 73736
  75.5 14.1 %collective-permute-start.9 = (f32[12,512]{1,0:T(8,128)S(1)}, f32[12,512]{1,0:T(8,128)S(1)}, u32[]{:S(2)}, u32[]{:S(2)}) collective-permute-start(f32[12,512]{1,0:T(8,128)S(1)} %slice.98), channel_id=1, source_target_pairs={{0,1},{1,2},{2,3},{4,5},{5,6},{6,7},{8,9},{9,10},{10,11},{12,13},{... | collective-permute-start | bytes 73736
  79.2 10.6 %collective-permute-start.7 = (f32[12,512]{1,0:T(8,128)S(1)}, f32[12,512]{1,0:T(8,128)S(1)}, u32[]{:S(2)}, u32[]{:S(2)}) collective-permute-start(f32[12,512]{1,0:T(8,128)S(1)} %slice.96), channel_id=1, source_target_pairs={{0,1},{1,2},{2,3},{4,5},{5,6},{6,7},{8,9},{9,10},{10,11},{12,13},{... | collective-permute-start | bytes 73736
  81.1 8.8 %collective-permute-start.10 = (f32[12,512]{1,0:T(8,128)S(1)}, f32[12,512]{1,0:T(8,128)S(1)}, u32[]{:S(2)}, u32[]{:S(2)}) collective-permute-start(f32[12,512]{1,0:T(8,128)S(1)} %slice.99), channel_id=1, source_target_pairs={{0,1},{1,2},{2,3},{4,5},{5,6},{6,7},{8,9},{9,10},{10,11},{12,13},{... | collective-permute-start | bytes 73736
  90.6 70.1 %copy-start.4 = (f32[2,28,4]{1,2,0:T(4,128)S(1)}, f32[2,28,4]{1,2,0:T(4,128)}, u32[]{:S(2)}) copy-start(f32[2,28,4]{1,2,0:T(4,128)} %param.25) | copy-start | bytes 2692
  90.6 70.1 %copy-start.5 = (f32[4]{0:T(128)S(1)}, f32[4]{0:T(128)}, u32[]{:S(2)}) copy-start(f32[4]{0:T(128)} %get-tuple-element.52) | copy-start | bytes 52
  175.5 10.0 %collective-permute-start.12 = (f32[12,512]{1,0:T(8,128)S(1)}, f32[12,512]{1,0:T(8,128)S(1)}, u32[]{:S(2)}, u32[]{:S(2)}) collective-permute-start(f32[12,512]{1,0:T(8,128)S(1)} %slice.101), channel_id=1, source_target_pairs={{0,1},{1,2},{2,3},{4,5},{5,6},{6,7},{8,9},{9,10},{10,11},{12,13},{... | collective-permute-start | bytes 73736
  176.8 8.9 %collective-permute-start.13 = (f32[12,512]{1,0:T(8,128)S(1)}, f32[12,512]{1,0:T(8,128)S(1)}, u32[]{:S(2)}, u32[]{:S(2)}) collective-permute-start(f32[12,512]{1,0:T(8,128)S(1)} %slice.102), channel_id=1, source_target_pairs={{0,1},{1,2},{2,3},{4,5},{5,6},{6,7},{8,9},{9,10},{10,11},{12,13},{... | collective-permute-start | bytes 73736
  180.6 5.2 %collective-permute-start.11 = (f32[12,512]{1,0:T(8,128)S(1)}, f32[12,512]{1,0:T(8,128)S(1)}, u32[]{:S(2)}, u32[]{:S(2)}) collective-permute-start(f32[12,512]{1,0:T(8,128)S(1)} %slice.100), channel_id=1, source_target_pairs={{0,1},{1,2},{2,3},{4,5},{5,6},{6,7},{8,9},{9,10},{10,11},{12,13},{... | collective-permute-start | bytes 73736
  182.5 3.5 %collective-permute-start.14 = (f32[12,512]{1,0:T(8,128)S(1)}, f32[12,512]{1,0:T(8,128)S(1)}, u32[]{:S(2)}, u32[]{:S(2)}) collective-permute-start(f32[12,512]{1,0:T(8,128)S(1)} %slice.103), channel_id=1, source_target_pairs={{0,1},{1,2},{2,3},{4,5},{5,6},{6,7},{8,9},{9,10},{10,11},{12,13},{... | collective-permute-start | bytes 73736
  186.5 14.4 %slice-start = ((s8[14680064]{0:T(1024)(128)(4,1)}), s8[2097152]{0:T(1024)(128)(4,1)S(1)}, s32[]{:S(2)}) async-start(s8[14680064]{0:T(1024)(128)(4,1)} %bitcast.132), calls=%async_computation | async-start | bytes 4194304
  186.8 14.1 %slice-start.1 = ((s8[14680064]{0:T(1024)(128)(4,1)}), s8[4194304]{0:T(1024)(128)(4,1)S(1)}, s32[]{:S(2)}) async-start(s8[14680064]{0:T(1024)(128)(4,1)} %bitcast.132), calls=%async_computation.1 | async-start | bytes 8388608
  186.8 14.1 %slice-start.2 = ((s8[14680064]{0:T(1024)(128)(4,1)}), s8[4194304]{0:T(1024)(128)(4,1)S(1)}, s32[]{:S(2)}) async-start(s8[14680064]{0:T(1024)(128)(4,1)} %bitcast.132), calls=%async_computation.2 | async-start | bytes 8388608
  186.8 14.1 %slice-start.3 = ((s8[14680064]{0:T(1024)(128)(4,1)}), s8[4194304]{0:T(1024)(128)(4,1)S(1)}, s32[]{:S(2)}) async-start(s8[14680064]{0:T(1024)(128)(4,1)} %bitcast.132), calls=%async_computation.3 | async-start | bytes 8388608
  200.9 7.4 %copy-start.2 = (f32[4,128]{1,0:T(4,128)S(1)}, f32[4,128]{1,0:T(4,128)}, u32[]{:S(2)}) copy-start(f32[4,128]{1,0:T(4,128)} %get-tuple-element.50) | copy-start | bytes 6148
  236.2 16.2 %collective-permute-start.15 = (bf16[14,1024]{1,0:T(8,128)(2,1)S(1)}, bf16[14,1024]{1,0:T(8,128)(2,1)S(1)}, u32[]{:S(2)}, u32[]{:S(2)}) collective-permute-start(bf16[14,1024]{1,0:T(8,128)(2,1)S(1)} %slice.104), channel_id=1, source_target_pairs={{0,4},{4,8},{8,12},{12,16},{16,20},{20,24},{24,28},{1,5},{5,9},{9,... | collective-permute-start | bytes 86024
